TPU v7x, 32 devices: a whole 2x2x4 slice. The times are simulated.
32 devices in a mesh: sp: 4 (over z), tp: 4 (over y, x), dp: 2 (over core).
Axes of the slice: x: 2, y: 2, z: 4, core: 2. Of those that a mesh axis runs over, the one named last changes fastest.
Arguments:
- latent: bfloat16 [2, 1024, 2048], P('dp', ('sp', 'tp')), may hold values from -6 to 6
- condition: bfloat16 [2, 2048], P('dp', ('sp', 'tp')), may hold values from -6 to 6
- context: bfloat16 [2, 32, 2048], P('dp', 'sp'), may hold values from -6 to 6
- context_vector: bfloat16 [2048], P(('sp', 'tp')), may hold values from -6 to 6
- modulator: bfloat16 [2048, 6144], P(('sp', 'tp')), may hold values from -0.3125 to 0.3125
- norm_gain: float32 [2048], replicated, may hold values from 0.1 to 1.9
- query_weight: bfloat16 [2048, 512], P(None, 'tp'), may hold values from -4 to 4
- key_weight: bfloat16 [2048, 512], P(None, 'tp'), may hold values from -0.125 to 0.125
- value_weight: bfloat16 [2048, 512], P(None, 'tp'), may hold values from -0.125 to 0.125
- head_gain: float32 [128], replicated, may hold values from 0.1 to 1.9
- lambdas: float32 [4], P('tp'), may hold values from 0.3 to 0.8
- context_bias: float32 [4, 2], P('tp'), may hold values from 1.3 to 2.7
- out_weight: bfloat16 [512, 2048], P('tp'), may hold values from -0.25 to 0.25
Outputs:
- updated: bfloat16 [2, 1024, 2048], P('dp', ('sp', 'tp'))
All inputs are finite; a program needn't handle non-finite values.
Results may differ from a plain program's by a relative error of at most 0.024.
Values may be sent and summed in bfloat16 or wider, within the bound.
A program may use at most 64 MiB of HBM per device.

v0:
```python
import jax
import jax.numpy as jnp
from jax import lax
from jax.sharding import PartitionSpec as P

EPSILON = 1e-06
OUT_SCALE = 0.8
KEY_BLOCK = 2048
LOW_START = -1e30


def modulate(inputs, gain_vector, shift_vector, scale_vector):
    as_float = inputs.astype(jnp.float32)
    normed = as_float * lax.rsqrt(jnp.mean(as_float * as_float, axis=-1, keepdims=True) + EPSILON)
    return (normed * gain_vector * (1.0 + scale_vector) + shift_vector).astype(jnp.bfloat16)


def fold_block(running, queries, keys_in, values_in, key_flags, bias_table, score_scale):
    run_max, run_total, summed = running
    scores = (
        jnp.einsum("qhmd,khmd->hmqk", queries, keys_in, preferred_element_type=jnp.float32)
        * score_scale
    )
    if key_flags is not None:
        scores = scores + bias_table[:, :, None, None] * key_flags
    new_max = jnp.maximum(run_max, jnp.max(scores, axis=-1))
    shrink = jnp.exp(run_max - new_max)
    weights = jnp.exp(scores - new_max[..., None])
    run_total = run_total * shrink + jnp.sum(weights, axis=-1)
    summed = summed * shrink[..., None] + jnp.einsum(
        "hmqk,khe->hmqe",
        weights.astype(jnp.bfloat16),
        values_in,
        preferred_element_type=jnp.float32,
    )
    return (new_max, run_total, summed)


def fold_keys(running, queries, keys_in, values_in, key_flags, bias_table, score_scale):
    full_blocks = keys_in.shape[0] // KEY_BLOCK
    if full_blocks > 1:
        edge = full_blocks * KEY_BLOCK
        stacked = (
            keys_in[:edge].reshape((full_blocks, KEY_BLOCK) + keys_in.shape[1:]),
            values_in[:edge].reshape((full_blocks, KEY_BLOCK) + values_in.shape[1:]),
        )
        if key_flags is not None:
            stacked = stacked + (key_flags[:edge].reshape(full_blocks, KEY_BLOCK),)

        def fold_step(current, block_data):
            flag_part = None if key_flags is None else block_data[2]
            return (
                fold_block(
                    current,
                    queries,
                    block_data[0],
                    block_data[1],
                    flag_part,
                    bias_table,
                    score_scale,
                ),
                None,
            )

        running, ignored = lax.scan(fold_step, running, stacked)
        keys_in = keys_in[edge:]
        values_in = values_in[edge:]
        key_flags = None if key_flags is None else key_flags[edge:]
    if keys_in.shape[0] > 0:
        running = fold_block(
            running, queries, keys_in, values_in, key_flags, bias_table, score_scale
        )
    return running


def body(
    latent,
    condition,
    context,
    context_vector,
    modulator,
    norm_gain,
    query_weight,
    key_weight,
    value_weight,
    head_gain,
    lambdas,
    context_bias,
    out_weight,
):
    model_width = latent.shape[2]
    local_heads = lambdas.shape[0]
    query_width = query_weight.shape[1]
    head_size = query_width // (2 * local_heads)
    value_size = value_weight.shape[1] // local_heads
    score_scale = head_size ** (-0.5)
    activated = jax.nn.silu(
        jnp.concatenate([condition, context_vector[None, :]], axis=0).astype(jnp.float32)
    )
    partial_terms = jnp.dot(
        activated.astype(jnp.bfloat16), modulator, preferred_element_type=jnp.float32
    )
    modulations = lax.psum(partial_terms, ("sp", "tp"))
    hidden = modulate(
        latent[0],
        norm_gain,
        modulations[0, :model_width],
        modulations[0, model_width : 2 * model_width],
    )
    ctx_hidden = modulate(
        context[0],
        norm_gain,
        modulations[1, :model_width],
        modulations[1, model_width : 2 * model_width],
    )
    gate_vector = modulations[0, 2 * model_width :]
    incoming = lax.all_gather(hidden, "tp", axis=0, tiled=True)
    projected = jnp.concatenate(
        [
            jnp.dot(incoming, query_weight, preferred_element_type=jnp.float32),
            jnp.dot(incoming, key_weight, preferred_element_type=jnp.float32),
            jnp.dot(incoming, value_weight, preferred_element_type=jnp.float32),
        ],
        axis=1,
    ).astype(jnp.bfloat16)
    query_rows = projected.shape[0]
    queries = projected[:, :query_width].reshape(query_rows, local_heads, 2, head_size)
    own_keys = projected[:, query_width : 2 * query_width]
    own_values = projected[:, 2 * query_width :]
    gathered_context = lax.all_gather(ctx_hidden, "sp", axis=0, tiled=True)
    ctx_keys = jnp.dot(gathered_context, key_weight, preferred_element_type=jnp.float32).astype(
        jnp.bfloat16
    )
    ctx_values = jnp.dot(gathered_context, value_weight, preferred_element_type=jnp.float32).astype(
        jnp.bfloat16
    )
    start_carry = (
        jnp.full((local_heads, 2, query_rows), LOW_START, jnp.float32),
        jnp.zeros((local_heads, 2, query_rows), jnp.float32),
        jnp.zeros((local_heads, 2, query_rows, value_size), jnp.float32),
    )
    pieces = (own_keys, own_values)
    initial = fold_keys(
        start_carry,
        queries,
        ctx_keys.reshape(-1, local_heads, 2, head_size),
        ctx_values.reshape(-1, local_heads, value_size),
        jnp.ones((ctx_keys.shape[0],), jnp.float32),
        context_bias,
        score_scale,
    )
    incoming = (
        lax.all_gather(pieces[0], "sp", axis=0, tiled=True),
        lax.all_gather(pieces[1], "sp", axis=0, tiled=True),
    )
    run_max, run_total, summed = fold_keys(
        initial,
        queries,
        incoming[0].reshape(-1, local_heads, 2, head_size),
        incoming[1].reshape(-1, local_heads, value_size),
        None,
        context_bias,
        score_scale,
    )
    mixed = (
        summed[:, 0] / run_total[:, 0, :, None]
        - lambdas[:, None, None] * summed[:, 1] / run_total[:, 1, :, None]
    )
    normed = (
        mixed
        * lax.rsqrt(jnp.mean(mixed * mixed, axis=-1, keepdims=True) + EPSILON)
        * head_gain
        * OUT_SCALE
    )
    attended = (
        jnp.transpose(normed, (1, 0, 2))
        .reshape(query_rows, local_heads * value_size)
        .astype(jnp.bfloat16)
    )
    exchanged = lax.all_to_all(attended, "tp", split_axis=0, concat_axis=1, tiled=True)
    whole_weight = lax.all_gather(out_weight, "tp", axis=0, tiled=True)
    branch = jnp.dot(exchanged, whole_weight, preferred_element_type=jnp.float32)
    result = (latent[0].astype(jnp.float32) + gate_vector * branch).astype(jnp.bfloat16)
    return result[None]


def solution(mesh):
    placed = (
        P("dp", ("sp", "tp"), None),
        P("dp", ("sp", "tp")),
        P("dp", "sp", None),
        P(("sp", "tp")),
        P(("sp", "tp"), None),
        P(),
        P(None, "tp"),
        P(None, "tp"),
        P(None, "tp"),
        P(),
        P("tp"),
        P("tp", None),
        P("tp", None),
    )
    return jax.shard_map(
        body, mesh=mesh, in_specs=placed, out_specs=P("dp", ("sp", "tp"), None), check_vma=False
    )
```

profile of v0, /device:TPU:0, one launch (start us, length us, event | category | flops | bytes accessed | tf_op | source)
XLA Modules:
  0.0 170.0 jit_solution(7644564545617815921)
XLA Ops:
  6.6 1.4 copy-done
  8.0 1.0 fusion.43
  9.0 78.7 %psum.7 = f32[2,6144]{1,0:T(2,128)S(1)} all-reduce(f32[2,6144]{1,0:T(2,128)S(1)} %fusion.43), channel_id=1, replica_groups=mesh['sp'=4,'tp'=4,'dp'=2] {'sp','tp'}, use_global_device_ids=true, to_apply=%region_0.1 | all-reduce | flops 12288 | bytes 98304 | tf_op jit(solution)/shard_map/psum | solution.py:103
  87.6 0.6 slice_add_fusion.1
  88.3 1.1 fusion.14
  89.4 1.6 fusion.18
  91.0 0.7 all-gather.5.cloned.1.call-update
  92.0 13.4 %all_gather.16 = bf16[32,2048]{1,0:T(8,128)(2,1)S(1)} all-gather(bf16[8,2048]{1,0:T(8,128)(2,1)S(1)} %fusion.27), channel_id=1, replica_groups=mesh['sp'=4,'tp'=4,'dp'=2] {'sp'}, dimensions={0}, use_global_device_ids=true | all-gather | bytes 163840 | tf_op jit(solution)/shard_map/all_gather | solution.py:130
  105.4 0.2 convolution_convert_fusion.4
  106.3 7.2 %all-gather.3.cloned.1.call-done = bf16[256,2048]{1,0:T(8,128)(2,1)} async-done(((bf16[64,2048]{1,0:T(8,128)(2,1)}), bf16[256,2048]{1,0:T(8,128)(2,1)}) %all-gather.3.cloned.1.call-update) | async-done | bytes 1048592 | tf_op jit(solution)/shard_map/all_gather | solution.py:117
  113.5 1.9 %convolution_convert_fusion.1 = bf16[256,128]{1,0:T(8,128)(2,1)S(1)} fusion(bf16[256,2048]{1,0:T(8,128)(2,1)} %all-gather.3.cloned.1.call-done, bf16[2048,128]{1,0:T(8,128)(2,1)} %param.20), kind=kOutput, calls=%fused_computation.13 | convolution fusion | flops 134250496 | bytes 1638400 | tf_op jit(solution)/shard_map/dot_general | solution.py:121
  115.4 14.6 %all_gather.17 = bf16[1024,128]{1,0:T(8,128)(2,1)} all-gather(bf16[256,128]{1,0:T(8,128)(2,1)S(1)} %convolution_convert_fusion.1), channel_id=1, replica_groups=mesh['sp'=4,'tp'=4,'dp'=2] {'sp'}, dimensions={0}, use_global_device_ids=true | all-gather | bytes 327680 | tf_op jit(solution)/shard_map/all_gather | solution.py:153
  130.0 1.8 %copy.30 = bf16[1024,128]{0,1:T(8,128)(2,1)} copy(bf16[1024,128]{1,0:T(8,128)(2,1)} %all_gather.17) | data formatting | bytes 524288 | tf_op jit(solution)/shard_map/all_gather | solution.py:153
  131.8 0.4 convolution_convert_fusion
  132.2 14.5 %all_gather.18 = bf16[1024,128]{1,0:T(8,128)(2,1)S(1)} all-gather(bf16[256,128]{1,0:T(8,128)(2,1)S(1)} %convolution_convert_fusion), channel_id=1, replica_groups=mesh['sp'=4,'tp'=4,'dp'=2] {'sp'}, dimensions={0}, use_global_device_ids=true | all-gather | bytes 327680 | tf_op jit(solution)/shard_map/all_gather | solution.py:154
  146.7 0.5 convolution_convert_fusion.2
  147.3 0.6 multiply_reduce_fusion
  147.9 1.3 copy-done.1
  149.2 0.5 fusion.10
  149.7 0.4 fusion.7
  150.2 2.1 %fusion.3 = f32[2,256]{1,0:T(2,128)S(1)} fusion(f32[2,256,1024]{2,1,0:T(8,128)} %copy-done.1, f32[2,256]{1,0:T(2,128)S(1)} %get-tuple-element.15), kind=kLoop, calls=%fused_computation.6 | loop fusion | flops 1572352 | bytes 2101248 | tf_op jit(solution)/shard_map/reduce_sum | solution.py:29
  152.3 0.2 fusion.22
  153.0 7.4 %all_to_all.16 = bf16[4,64,128]{2,1,0:T(8,128)(2,1)S(1)} all-to-all(bf16[4,64,128]{2,1,0:T(8,128)(2,1)S(1)} %multiply_convert_fusion), channel_id=1, replica_groups=mesh['sp'=4,'tp'=4,'dp'=2] {'tp'}, dimensions={0} | all-to-all | bytes 131072 | tf_op jit(solution)/shard_map/all_to_all | solution.py:180
  160.4 2.8 %fusion.2 = bf16[1,64,2048]{2,1,0:T(8,128)(2,1)} fusion(bf16[512,2048]{1,0:T(8,128)(2,1)} %all-gather.5.cloned.1.call-done, bf16[1,64,2048]{2,1,0:T(8,128)(2,1)S(1)} %copy-done.3, f32[2048]{0:T(1024)S(1)} %bitcast.94, bf16[4,64,128]{2,1,0:T(8,128)(2,1)S(1)} %all_to_all.16), kind=kOutput, calls=%fused_computation.3 | convolution fusion | flops 134742016 | bytes 2695168 | tf_op jit(solution)/shard_map/dot_general | solution.py:182
  (44 shorter events, 1.1 us)
Async XLA Ops:
  6.5 1.4 copy-start
  6.5 82.8 %copy-start.3 = (bf16[1,64,2048]{2,1,0:T(8,128)(2,1)S(1)}, bf16[1,64,2048]{2,1,0:T(8,128)(2,1)}, u32[]{:S(2)}) copy-start(bf16[1,64,2048]{2,1,0:T(8,128)(2,1)} %param.13) | copy-start | bytes 786436
  6.5 85.4 %copy-start.10 = (f32[2048]{0:T(1024)S(1)}, f32[2048]{0:T(1024)}, u32[]{:S(2)}) copy-start(f32[2048]{0:T(1024)} %param.18) | copy-start | bytes 24580
  6.5 85.2 %copy-start.8 = (bf16[1,8,2048]{2,1,0:T(8,128)(2,1)S(1)}, bf16[1,8,2048]{2,1,0:T(8,128)(2,1)}, u32[]{:S(2)}) copy-start(bf16[1,8,2048]{2,1,0:T(8,128)(2,1)} %param.15) | copy-start | bytes 98308
  6.5 98.8 %copy-start.5 = (bf16[2048,128]{1,0:T(8,128)(2,1)S(1)}, bf16[2048,128]{1,0:T(8,128)(2,1)}, u32[]{:S(2)}) copy-start(bf16[2048,128]{1,0:T(8,128)(2,1)} %param.20) | copy-start | bytes 1572868
  6.6 107.0 %all-gather.3.cloned.1.call-start = ((), (), s32[]{:S(2)}) async-start(), calls=%async_computation.1 | async-start | bytes 1310720 | tf_op jit(solution)/shard_map/all_gather | solution.py:117
  91.0 40.8 %copy-start.4 = (bf16[2048,128]{1,0:T(8,128)(2,1)S(1)}, bf16[2048,128]{1,0:T(8,128)(2,1)}, u32[]{:S(2)}) copy-start(bf16[2048,128]{1,0:T(8,128)(2,1)} %param.21) | copy-start | bytes 1572868
  91.0 69.4 %all-gather.5.cloned.1.call-start = ((), (), s32[]{:S(2)}) async-start(), calls=%async_computation.2 | async-start | bytes 2621440 | tf_op jit(solution)/shard_map/all_gather | solution.py:181
  113.5 18.3 %copy-start.2 = (bf16[256,2048]{1,0:T(8,128)(2,1)S(1)}, bf16[256,2048]{1,0:T(8,128)(2,1)}, u32[]{:S(2)}) copy-start(bf16[256,2048]{1,0:T(8,128)(2,1)} %all-gather.3.cloned.1.call-done) | copy-start | bytes 3145732
  131.8 14.9 %copy-start.7 = (bf16[2048,128]{1,0:T(8,128)(2,1)S(1)}, bf16[2048,128]{1,0:T(8,128)(2,1)}, u32[]{:S(2)}) copy-start(bf16[2048,128]{1,0:T(8,128)(2,1)} %param.19) | copy-start | bytes 1572868
  131.8 15.4 %copy-start.11 = (f32[1,2]{1,0:T(1,128)S(1)}, f32[1,2]{1,0:T(1,128)}, u32[]{:S(2)}) copy-start(f32[1,2]{1,0:T(1,128)} %param.24) | copy-start | bytes 28
  131.8 15.6 %copy-start.6 = (bf16[1024,128]{0,1:T(8,128)(2,1)S(1)}, bf16[1024,128]{0,1:T(8,128)(2,1)}, u32[]{:S(2)}) copy-start(bf16[1024,128]{0,1:T(8,128)(2,1)} %copy.30) | copy-start | bytes 786436
  147.9 1.3 copy-start.1
  149.7 3.1 %copy-start.12 = (f32[128]{0:T(128)S(1)}, f32[128]{0:T(128)}, u32[]{:S(2)}) copy-start(f32[128]{0:T(128)} %param.22) | copy-start | bytes 1540
  149.7 10.6 %copy-start.9 = (f32[1,2048]{1,0:T(1,128)S(1)}, f32[1,2048]{1,0:T(1,128)}, u32[]{:S(2)}) copy-start(f32[1,2048]{1,0:T(1,128)} %get-tuple-element.13) | copy-start | bytes 24580
Sparse Core Ops, SparseCore 0:
  91.1 22.3 all-gather.2
  115.3 35.1 all-gather.4
where the time goes:
time: 170 us
  blocking collectives  129 us (76%)
  between operations  14.3 us (8%)
  matrix products  8.34 us (5%)
  waiting for transfers between devices  7.88 us (5%)
  other arithmetic  6.08 us (4%)
  local copies, waits for them, and re-layouts  4.84 us (3%)
    psum x1, blocking collectives, body(): modulations = lax.psum(partial_terms, ('sp', 'tp'))  78.7 us
    all_gather x1, blocking collectives, body(): lax.all_gather(pieces[0], 'sp', axis=0, tiled=True)  14.6 us
    all_gather x1, blocking collectives, body(): lax.all_gather(pieces[1], 'sp', axis=0, tiled=True)  14.5 us
    all_gather x1, blocking collectives, body(): gathered_context = lax.all_gather(ctx_hidden, 'sp', axis=0, tiled=True)  13.4 us
    all_to_all x1, blocking collectives, body(): lax.all_to_all(attended, 'tp', split_axis=0, concat_axis=1, tiled=True)  7.38 us
    all_gather x1, waiting for transfers between devices, body(): incoming = lax.all_gather(hidden, 'tp', axis=0, tiled=True)  7.17 us
  transfers between devices with their start and end apart: 2, of which 1 were waited for; matrix products, arithmetic and copies ran while one was open for 6% of the time, Pallas kernels for 0%

commit v1 on v0

--- a/solution.py
+++ b/solution.py
@@ -100,7 +100,8 @@
     partial_terms = jnp.dot(
         activated.astype(jnp.bfloat16), modulator, preferred_element_type=jnp.float32
     )
-    modulations = lax.psum(partial_terms, ("sp", "tp"))
+    long_array = lax.all_gather(partial_terms, axis_name=("sp", "tp"))
+    modulations = jnp.sum(long_array, axis=0)
     hidden = modulate(
         latent[0],
         norm_gain,

time: 170 us -> 138 us (0.81)
  blocking collectives: 129 us -> 97.1 us
    psum x1 -> x0, blocking collectives: 78.7 us -> none  [body(): modulations = lax.psum(partial_terms, ('sp', 'tp'))]
    all_gather x0 -> x1, blocking collectives: none -> 47.2 us  [body(): long_array = lax.all_gather(partial_terms, axis_name=('sp', 'tp'))]
  transfers between devices with their start and end apart: 2 -> 2, of which waited for: 1 -> 1; matrix products, arithmetic and copies ran while one was open for 6% -> 7% of each run, Pallas kernels for 0% -> 0%
where the time goes in v1:
time: 138 us; the launch traced here: 137 us
  blocking collectives  97.1 us (70%)
  between operations  14.2 us (10%)
  matrix products  8.34 us (6%)
  waiting for transfers between devices  7.88 us (6%)
  local copies, waits for them, and re-layouts  4.87 us (4%)
  other arithmetic  4.69 us (3%)
    all_gather x1, blocking collectives, body(): long_array = lax.all_gather(partial_terms, axis_name=('sp', 'tp'))  47.2 us
    all_gather x1, blocking collectives, body(): lax.all_gather(pieces[0], 'sp', axis=0, tiled=True)  14.6 us
    all_gather x1, blocking collectives, body(): lax.all_gather(pieces[1], 'sp', axis=0, tiled=True)  14.4 us
    all_gather x1, blocking collectives, body(): gathered_context = lax.all_gather(ctx_hidden, 'sp', axis=0, tiled=True)  13.4 us
    all_to_all x1, blocking collectives, body(): lax.all_to_all(attended, 'tp', split_axis=0, concat_axis=1, tiled=True)  7.41 us
    all_gather x1, waiting for transfers between devices, body(): incoming = lax.all_gather(hidden, 'tp', axis=0, tiled=True)  7.17 us
    dot_general x1, matrix products, body(): jnp.dot(exchanged, whole_weight, preferred_element_type=jnp.float32)  2.78 us
  transfers between devices with their start and end apart: 2, of which 1 were waited for; matrix products, arithmetic and copies ran while one was open for 7% of the time, Pallas kernels for 0%

profile of v1, /device:TPU:0, one launch (start us, length us, event | category | flops | bytes accessed | tf_op | source)
XLA Modules:
  0.0 137.1 jit_solution(15674720366132445127)
XLA Ops:
  6.5 1.4 %copy-done = bf16[128,6144]{1,0:T(8,128)(2,1)S(1)} copy-done((bf16[128,6144]{1,0:T(8,128)(2,1)S(1)}, bf16[128,6144]{1,0:T(8,128)(2,1)}, u32[]{:S(2)}) %copy-start) | copy-done | bytes 1572888
  7.9 1.0 convolution_bitcast_fusion
  9.0 47.2 %all-gather.1 = f32[16,2,6144]{2,1,0:T(2,128)S(1)} all-gather(f32[1,2,6144]{2,1,0:T(2,128)S(1)} %convolution_bitcast_fusion), channel_id=2, replica_groups=mesh['sp'=4,'tp'=4,'dp'=2] {'sp','tp'}, dimensions={0}, use_global_device_ids=true | all-gather | bytes 835584 | tf_op jit(solution)/shard_map/all_gather | solution.py:103
  56.2 0.3 reduce_sum.58
  56.4 0.6 slice_add_fusion.1
  57.2 0.9 fusion.18
  58.2 0.7 all-gather.7.cloned.1.call-update
  59.1 13.4 %all_gather.24 = bf16[32,2048]{1,0:T(8,128)(2,1)S(1)} all-gather(bf16[8,2048]{1,0:T(8,128)(2,1)S(1)} %fusion.27), channel_id=1, replica_groups=mesh['sp'=4,'tp'=4,'dp'=2] {'sp'}, dimensions={0}, use_global_device_ids=true | all-gather | bytes 163840 | tf_op jit(solution)/shard_map/all_gather | solution.py:131
  72.5 0.2 convolution_convert_fusion.4
  73.5 7.2 %all-gather.5.cloned.1.call-done = bf16[256,2048]{1,0:T(8,128)(2,1)} async-done(((bf16[64,2048]{1,0:T(8,128)(2,1)}), bf16[256,2048]{1,0:T(8,128)(2,1)}) %all-gather.5.cloned.1.call-update) | async-done | bytes 1048592 | tf_op jit(solution)/shard_map/all_gather | solution.py:118
  80.7 1.9 %convolution_convert_fusion.1 = bf16[256,128]{1,0:T(8,128)(2,1)S(1)} fusion(bf16[256,2048]{1,0:T(8,128)(2,1)} %all-gather.5.cloned.1.call-done, bf16[2048,128]{1,0:T(8,128)(2,1)} %param.20), kind=kOutput, calls=%fused_computation.14 | convolution fusion | flops 134250496 | bytes 1638400 | tf_op jit(solution)/shard_map/dot_general | solution.py:122
  82.5 14.6 %all_gather.25 = bf16[1024,128]{1,0:T(8,128)(2,1)} all-gather(bf16[256,128]{1,0:T(8,128)(2,1)S(1)} %convolution_convert_fusion.1), channel_id=1, replica_groups=mesh['sp'=4,'tp'=4,'dp'=2] {'sp'}, dimensions={0}, use_global_device_ids=true | all-gather | bytes 327680 | tf_op jit(solution)/shard_map/all_gather | solution.py:154
  97.1 1.8 %copy.30 = bf16[1024,128]{0,1:T(8,128)(2,1)} copy(bf16[1024,128]{1,0:T(8,128)(2,1)} %all_gather.25) | data formatting | bytes 524288 | tf_op jit(solution)/shard_map/all_gather | solution.py:154
  98.9 0.4 convolution_convert_fusion
  99.4 14.4 %all_gather.26 = bf16[1024,128]{1,0:T(8,128)(2,1)S(1)} all-gather(bf16[256,128]{1,0:T(8,128)(2,1)S(1)} %convolution_convert_fusion), channel_id=1, replica_groups=mesh['sp'=4,'tp'=4,'dp'=2] {'sp'}, dimensions={0}, use_global_device_ids=true | all-gather | bytes 327680 | tf_op jit(solution)/shard_map/all_gather | solution.py:155
  113.8 0.5 convolution_convert_fusion.2
  114.5 0.6 multiply_reduce_fusion
  115.0 1.3 copy-done.1
  116.3 0.5 fusion.10
  116.9 0.4 fusion.7
  117.3 2.1 %fusion.3 = f32[2,256]{1,0:T(2,128)S(1)} fusion(f32[2,256,1024]{2,1,0:T(8,128)} %copy-done.1, f32[2,256]{1,0:T(2,128)S(1)} %get-tuple-element.15), kind=kLoop, calls=%fused_computation.7 | loop fusion | flops 1572352 | bytes 2101248 | tf_op jit(solution)/shard_map/reduce_sum | solution.py:29
  119.4 0.2 fusion.22
  120.1 7.4 %all_to_all.16 = bf16[4,64,128]{2,1,0:T(8,128)(2,1)S(1)} all-to-all(bf16[4,64,128]{2,1,0:T(8,128)(2,1)S(1)} %multiply_convert_fusion), channel_id=1, replica_groups=mesh['sp'=4,'tp'=4,'dp'=2] {'tp'}, dimensions={0} | all-to-all | bytes 131072 | tf_op jit(solution)/shard_map/all_to_all | solution.py:181
  127.5 2.8 %fusion.2 = bf16[1,64,2048]{2,1,0:T(8,128)(2,1)} fusion(bf16[512,2048]{1,0:T(8,128)(2,1)} %all-gather.7.cloned.1.call-done, bf16[1,64,2048]{2,1,0:T(8,128)(2,1)S(1)} %copy-done.3, f32[2048]{0:T(1024)S(1)} %bitcast.96, bf16[4,64,128]{2,1,0:T(8,128)(2,1)S(1)} %all_to_all.16), kind=kOutput, calls=%fused_computation.4 | convolution fusion | flops 134742016 | bytes 2695168 | tf_op jit(solution)/shard_map/dot_general | solution.py:183
  (45 shorter events, 1.3 us)
Async XLA Ops:
  6.5 1.4 %copy-start = (bf16[128,6144]{1,0:T(8,128)(2,1)S(1)}, bf16[128,6144]{1,0:T(8,128)(2,1)}, u32[]{:S(2)}) copy-start(bf16[128,6144]{1,0:T(8,128)(2,1)} %param.17) | copy-start | bytes 4718596
  6.5 50.5 %copy-start.3 = (bf16[1,64,2048]{2,1,0:T(8,128)(2,1)S(1)}, bf16[1,64,2048]{2,1,0:T(8,128)(2,1)}, u32[]{:S(2)}) copy-start(bf16[1,64,2048]{2,1,0:T(8,128)(2,1)} %param.13) | copy-start | bytes 786436
  6.5 50.7 %copy-start.10 = (f32[2048]{0:T(1024)S(1)}, f32[2048]{0:T(1024)}, u32[]{:S(2)}) copy-start(f32[2048]{0:T(1024)} %param.18) | copy-start | bytes 24580
  6.5 74.1 %all-gather.5.cloned.1.call-start = ((), (), s32[]{:S(2)}) async-start(), calls=%async_computation.1 | async-start | bytes 1310720 | tf_op jit(solution)/shard_map/all_gather | solution.py:118
  7.9 51.0 %copy-start.8 = (bf16[1,8,2048]{2,1,0:T(8,128)(2,1)S(1)}, bf16[1,8,2048]{2,1,0:T(8,128)(2,1)}, u32[]{:S(2)}) copy-start(bf16[1,8,2048]{2,1,0:T(8,128)(2,1)} %param.15) | copy-start | bytes 98308
  8.9 63.6 %copy-start.5 = (bf16[2048,128]{1,0:T(8,128)(2,1)S(1)}, bf16[2048,128]{1,0:T(8,128)(2,1)}, u32[]{:S(2)}) copy-start(bf16[2048,128]{1,0:T(8,128)(2,1)} %param.20) | copy-start | bytes 1572868
  58.1 40.8 %copy-start.4 = (bf16[2048,128]{1,0:T(8,128)(2,1)S(1)}, bf16[2048,128]{1,0:T(8,128)(2,1)}, u32[]{:S(2)}) copy-start(bf16[2048,128]{1,0:T(8,128)(2,1)} %param.21) | copy-start | bytes 1572868
  58.1 69.4 %all-gather.7.cloned.1.call-start = ((), (), s32[]{:S(2)}) async-start(), calls=%async_computation.2 | async-start | bytes 2621440 | tf_op jit(solution)/shard_map/all_gather | solution.py:182
  80.7 18.3 %copy-start.2 = (bf16[256,2048]{1,0:T(8,128)(2,1)S(1)}, bf16[256,2048]{1,0:T(8,128)(2,1)}, u32[]{:S(2)}) copy-start(bf16[256,2048]{1,0:T(8,128)(2,1)} %all-gather.5.cloned.1.call-done) | copy-start | bytes 3145732
  98.9 14.9 %copy-start.7 = (bf16[2048,128]{1,0:T(8,128)(2,1)S(1)}, bf16[2048,128]{1,0:T(8,128)(2,1)}, u32[]{:S(2)}) copy-start(bf16[2048,128]{1,0:T(8,128)(2,1)} %param.19) | copy-start | bytes 1572868
  98.9 15.4 %copy-start.11 = (f32[1,2]{1,0:T(1,128)S(1)}, f32[1,2]{1,0:T(1,128)}, u32[]{:S(2)}) copy-start(f32[1,2]{1,0:T(1,128)} %param.24) | copy-start | bytes 28
  98.9 15.5 %copy-start.6 = (bf16[1024,128]{0,1:T(8,128)(2,1)S(1)}, bf16[1024,128]{0,1:T(8,128)(2,1)}, u32[]{:S(2)}) copy-start(bf16[1024,128]{0,1:T(8,128)(2,1)} %copy.30) | copy-start | bytes 786436
  115.0 1.3 copy-start.1
  116.9 3.1 %copy-start.12 = (f32[128]{0:T(128)S(1)}, f32[128]{0:T(128)}, u32[]{:S(2)}) copy-start(f32[128]{0:T(128)} %param.22) | copy-start | bytes 1540
  116.9 10.7 %copy-start.9 = (f32[1,2048]{1,0:T(1,128)S(1)}, f32[1,2048]{1,0:T(1,128)}, u32[]{:S(2)}) copy-start(f32[1,2048]{1,0:T(1,128)} %get-tuple-element.13) | copy-start | bytes 24580
Sparse Core Ops, SparseCore 0:
  58.3 22.3 all-gather.4
  82.5 35.1 all-gather.6
